TPU v7x, 32 devices: a whole 2x2x4 slice. The times are simulated.
32 devices in a mesh: sp: 8 (over z, y), tp: 4 (over x, core).
Axes of the slice: x: 2, y: 2, z: 4, core: 2. Of those that a mesh axis runs over, the one named last changes fastest.
Arguments:
- resid_in: bfloat16 [1024, 2048], P('sp'), may hold values from -6 to 6
- query_plain: bfloat16 [1024, 2048], P('sp', 'tp'), may hold values from -480 to 480, as said below
- query_turn: bfloat16 [1024, 1024], P('sp', 'tp'), may hold values from -16 to 16
- latent_raw: bfloat16 [1024, 256], P('sp'), may hold values from -6 to 6
- shared_key: bfloat16 [1024, 32], P('sp'), may hold values from -6 to 6
- latent_gain: float32 [256], replicated, may hold values from 0.1 to 1.9
- key_up: bfloat16 [256, 2048], P(None, 'tp'), may hold values from -0.375 to 0.375
- value_up: bfloat16 [256, 2048], P(None, 'tp'), may hold values from -0.375 to 0.375
- out_weight: bfloat16 [2048, 2048], P('tp'), may hold values from -0.5 to 0.5
- mixer_gain: float32 [2048], replicated, may hold values from 0.1 to 1.9
- gate_weight: bfloat16 [2048, 5632], P('sp', 'tp'), may hold values from -0.125 to 0.125
- up_weight: bfloat16 [2048, 5632], P('sp', 'tp'), may hold values from -0.125 to 0.125
- down_weight: bfloat16 [5632, 2048], P('tp', 'sp'), may hold values from -0.15625 to 0.15625
Outputs:
- layer_out: bfloat16 [1024, 2048], P(('sp', 'tp'))
Inputs may be any that keep to these rules, and one draw needn't show every extreme that they name: Entries of query_plain lie in this range.
All inputs are finite; a program needn't handle non-finite values.
Results may differ from a plain program's by a relative error of at most 0.014.
The roundings to bfloat16 on the way count: a program that leaves them out, or rounds other values in their place, can miss the bound.
Values may be sent and summed in bfloat16 or wider, within the bound.
A program may use at most 128 MiB of HBM per device.

v0:
```python
import math

import jax
import jax.numpy as jnp
from jax import lax
from jax.sharding import PartitionSpec as P

NOPE = 64
ROPE = 32
V = 64


def rotate(values, cosine, sine):
    half_width = values.shape[-1] // 2
    first = values[..., :half_width]
    second = values[..., half_width:]
    return jnp.concatenate(
        [first * cosine - second * sine, first * sine + second * cosine], axis=-1
    )


def rms_scale(values, gain):
    return values * lax.rsqrt(jnp.mean(values * values, axis=-1, keepdims=True) + 1e-06) * gain


def per_device(
    resid_in,
    query_plain,
    query_turn,
    latent_raw,
    shared_key,
    latent_gain,
    key_up,
    value_up,
    out_weight,
    mixer_gain,
    gate_weight,
    up_weight,
    down_weight,
):
    tok_rows = resid_in.shape[0]
    head_count = query_plain.shape[1] // NOPE
    part_rows = tok_rows // lax.axis_size("tp")
    offset = lax.axis_index("sp") * tok_rows
    position = (offset + jnp.arange(tok_rows, dtype=jnp.int32)).astype(jnp.float32)
    inverse = 10000.0 ** (-jnp.arange(0, ROPE, 2, dtype=jnp.float32) / ROPE)
    angles = position[:, None] * inverse[None, :]
    cosine = jnp.cos(angles)
    sine = jnp.sin(angles)
    query_heads = query_plain.reshape(tok_rows, head_count, NOPE)
    query_rot = rotate(
        query_turn.reshape(tok_rows, head_count, ROPE).astype(jnp.float32),
        cosine[:, None, :],
        sine[:, None, :],
    ).astype(jnp.bfloat16)
    latent = rms_scale(latent_raw.astype(jnp.float32), latent_gain).astype(jnp.bfloat16)
    key_rot = rotate(shared_key.astype(jnp.float32), cosine, sine).astype(jnp.bfloat16)
    softmax_scale = (NOPE + ROPE) ** (-0.5)

    def attend_block(state, key_plain, values, key_pos):
        run_max, run_total, run_acc = state
        score = jnp.einsum(
            "qhd,khd->hqk", query_heads, key_plain, preferred_element_type=jnp.float32
        )
        score = score + jnp.einsum(
            "qhr,kr->hqk", query_rot, key_pos, preferred_element_type=jnp.float32
        )
        score = score * softmax_scale
        new_max = jnp.maximum(run_max, jnp.max(score, axis=-1))
        shrink = jnp.exp(run_max - new_max)
        expo = jnp.exp(score - new_max[:, :, None])
        run_total = run_total * shrink + jnp.sum(expo, axis=-1)
        run_acc = run_acc * shrink.T[:, :, None] + jnp.einsum(
            "hqk,khd->qhd", expo.astype(jnp.bfloat16), values, preferred_element_type=jnp.float32
        )
        return (new_max, run_total, run_acc)

    start_state = (
        jnp.full((head_count, tok_rows), -jnp.inf, jnp.float32),
        jnp.zeros((head_count, tok_rows), jnp.float32),
        jnp.zeros((tok_rows, head_count, V), jnp.float32),
    )
    state = start_state
    latent_piece = lax.all_gather(latent, "sp", axis=0, tiled=True)
    pos_piece = lax.all_gather(key_rot, "sp", axis=0, tiled=True)
    piece_len = latent_piece.shape[0]
    block_len = math.gcd(piece_len, 512)
    block_count = piece_len // block_len

    def one_block(inner, items):
        latent_rows, pos_rows = items
        key_plain = (
            jnp.dot(latent_rows, key_up, preferred_element_type=jnp.float32)
            .astype(jnp.bfloat16)
            .reshape(block_len, head_count, NOPE)
        )
        values = (
            jnp.dot(latent_rows, value_up, preferred_element_type=jnp.float32)
            .astype(jnp.bfloat16)
            .reshape(block_len, head_count, V)
        )
        return (attend_block(inner, key_plain, values, pos_rows), None)

    state, unused = lax.scan(
        one_block,
        state,
        (
            latent_piece.reshape(block_count, block_len, latent_piece.shape[1]),
            pos_piece.reshape(block_count, block_len, ROPE),
        ),
    )
    attended = (
        (state[2] / state[1].T[:, :, None]).astype(jnp.bfloat16).reshape(tok_rows, head_count * V)
    )
    own_start = lax.axis_index("tp") * part_rows
    mixed = lax.psum_scatter(
        jnp.dot(attended, out_weight, preferred_element_type=jnp.float32).astype(jnp.bfloat16),
        "tp",
        scatter_dimension=0,
        tiled=True,
    ).astype(jnp.float32)
    middle = lax.dynamic_slice_in_dim(resid_in, own_start, part_rows, 0).astype(jnp.float32) + mixed
    normed = rms_scale(middle, mixer_gain).astype(jnp.bfloat16)
    all_rows = lax.all_gather(normed, "tp", axis=0, tiled=True)
    gate_sum = jnp.dot(
        all_rows,
        lax.all_gather(gate_weight, "sp", axis=0, tiled=True),
        preferred_element_type=jnp.float32,
    )
    up_sum = jnp.dot(
        all_rows,
        lax.all_gather(up_weight, "sp", axis=0, tiled=True),
        preferred_element_type=jnp.float32,
    )
    hidden = (jax.nn.silu(gate_sum) * up_sum).astype(jnp.bfloat16)
    terms = jnp.dot(
        hidden,
        lax.all_gather(down_weight, "sp", axis=1, tiled=True),
        preferred_element_type=jnp.float32,
    )
    down_sum = lax.psum_scatter(
        terms.astype(jnp.bfloat16), "tp", scatter_dimension=0, tiled=True
    ).astype(jnp.float32)
    return (middle + 0.5 * down_sum).astype(jnp.bfloat16)


def solution(mesh):
    return jax.shard_map(
        per_device,
        mesh=mesh,
        in_specs=(
            P("sp", None),
            P("sp", "tp"),
            P("sp", "tp"),
            P("sp", None),
            P("sp", None),
            P(),
            P(None, "tp"),
            P(None, "tp"),
            P("tp", None),
            P(),
            P("sp", "tp"),
            P("sp", "tp"),
            P("tp", "sp"),
        ),
        out_specs=P(("sp", "tp"), None),
        check_vma=False,
    )
```

profile of v0, /device:TPU:0, one launch (start us, length us, event | category | flops | bytes accessed | tf_op | source)
XLA Modules:
  0.0 402.0 jit_solution(11615613953259586742)
XLA Ops:
  7.4 0.0 copy-start
  7.4 0.0 reduce-scatter.3.cloned.1.call-start
  7.4 0.8 convert_element_type.63
  8.3 0.9 copy.19
  9.2 0.1 multiply_cosine_fusion
  9.3 27.8 %all_gather.19 = bf16[1024,32]{0,1:T(8,128)(2,1)S(1)} all-gather(bf16[128,32]{0,1:T(8,128)(2,1)S(1)} %pad_maximum_fusion.1), channel_id=1, replica_groups=mesh['sp'=8,'tp'=4] {'sp'}, dimensions={0}, use_global_device_ids=true | all-gather | bytes 73728 | tf_op jit(solution)/shard_map/all_gather | solution.py:85
  37.1 0.9 fusion.19
  38.1 0.9 fusion.21
  39.0 31.3 %all_gather.18 = bf16[1024,256]{1,0:T(8,128)(2,1)S(1)} all-gather(bf16[128,256]{1,0:T(8,128)(2,1)S(1)} %fusion.21), channel_id=1, replica_groups=mesh['sp'=8,'tp'=4] {'sp'}, dimensions={0}, use_global_device_ids=true | all-gather | bytes 589824 | tf_op jit(solution)/shard_map/all_gather | solution.py:84
  70.4 1.0 copy.18
  71.5 13.4 %while.15 = (s32[]{:T(128)}, f32[8,128]{1,0:T(8,128)S(1)}, f32[8,128]{1,0:T(8,128)S(1)}, f32[128,8,64]{0,2,1:T(8,128)S(1)}, bf16[2,512,256]{2,1,0:T(8,128)(2,1)S...) while((s32[]{:T(128)}, f32[8,128]{1,0:T(8,128)S(1)}, ...), condition=%wide.region_4.5_spmd.clone, body=%wide.region_1.4_spmd.clone.sunk | while | flops 440604672 | bytes 23888068 | solution.py:104
  71.5 1.3 convolution_convert_fusion.6
  72.8 0.5 fusion.63
  73.3 0.0 copy-start.2
  73.3 1.8 fusion.64
  75.1 0.3 convolution_convert_fusion.7
  75.5 2.3 fusion.68
  77.8 0.3 fusion.66
  78.2 1.3 convolution_convert_fusion.6
  79.5 0.5 fusion.63
  80.0 0.0 copy-start.2
  80.0 1.8 fusion.64
  81.8 0.3 convolution_convert_fusion.7
  82.2 2.3 fusion.68
  84.5 0.3 fusion.66
  84.9 0.0 copy-done
  84.9 0.0 copy-start.4
  84.9 1.3 convolution_convert_fusion.2
  86.2 0.0 reduce-scatter.3.cloned.1.call-update
  86.2 0.0 all-gather.4.cloned.1.call-start
  86.3 0.5 all-gather.4.cloned.1.call-update
  86.8 0.0 all-gather.6.cloned.1.call-start
  86.8 0.5 all-gather.6.cloned.1.call-update
  87.4 0.0 all-gather.8.cloned.1.call-start
  87.4 0.5 all-gather.8.cloned.1.call-update
  88.0 0.0 reduce-scatter.5.cloned.1.call-start
  88.0 19.3 %reduce-scatter.3.cloned.1.call-done = bf16[32,2048]{1,0:T(8,128)(2,1)} async-done(((bf16[128,2048]{1,0:T(8,128)(2,1)}), bf16[32,2048]{1,0:T(8,128)(2,1)}) %reduce-scatter.3.cloned.1.call-update) | async-done | bytes 131088 | tf_op jit(solution)/shard_map/reduce_scatter | solution.py:116
  107.3 1.1 multiply_reduce_fusion
  108.4 1.0 multiply_convert_fusion
  109.4 6.6 %all_gather.20 = bf16[128,2048]{1,0:T(8,128)(2,1)S(1)} all-gather(bf16[32,2048]{1,0:T(8,128)(2,1)S(1)} %multiply_convert_fusion), channel_id=1, replica_groups=mesh['sp'=8,'tp'=4] {'tp'}, dimensions={0}, use_global_device_ids=true | all-gather | bytes 655360 | tf_op jit(solution)/shard_map/all_gather | solution.py:124
  116.0 64.3 %all-gather.4.cloned.1.call-done = bf16[2048,1408]{1,0:T(8,128)(2,1)} async-done(((bf16[256,1408]{1,0:T(8,128)(2,1)}), bf16[2048,1408]{1,0:T(8,128)(2,1)}) %all-gather.4.cloned.1.call-update) | async-done | bytes 5767184 | tf_op jit(solution)/shard_map/all_gather | solution.py:127
  180.3 3.6 fusion.25
  184.0 88.7 %all-gather.6.cloned.1.call-done = bf16[2048,1408]{1,0:T(8,128)(2,1)} async-done(((bf16[256,1408]{1,0:T(8,128)(2,1)}), bf16[2048,1408]{1,0:T(8,128)(2,1)}) %all-gather.6.cloned.1.call-update) | async-done | bytes 5767184 | tf_op jit(solution)/shard_map/all_gather | solution.py:132
  272.7 93.0 %all-gather.8.cloned.1.call-done = bf16[1408,2048]{1,0:T(8,128)(2,1)} async-done(((bf16[1408,256]{1,0:T(8,128)(2,1)}), bf16[1408,2048]{1,0:T(8,128)(2,1)}) %all-gather.8.cloned.1.call-update) | async-done | bytes 5767184 | tf_op jit(solution)/shard_map/all_gather | solution.py:138
  365.7 7.1 %convolution_convert_fusion.3 = bf16[128,2048]{1,0:T(8,128)(2,1)} fusion(bf16[1408,2048]{1,0:T(8,128)(2,1)} %all-gather.8.cloned.1.call-done, bf16[128,2048]{1,0:T(8,128)(2,1)S(1)} %all_gather.20, bf16[2048,1408]{1,0:T(8,128)(2,1)} %all-gather.6.cloned.1.call-done, f32[128,1408]{1,0:T(8,128)S(1)} %fusion.25), kind=kOutput, calls=%fused_computation.28 | convolution fusion | flops 1477738496 | bytes 13303808 | tf_op jit(solution)/shard_map/dot_general | solution.py:136
  372.7 0.0 reduce-scatter.5.cloned.1.call-update
  372.7 20.0 %reduce-scatter.5.cloned.1.call-done = bf16[32,2048]{1,0:T(8,128)(2,1)} async-done(((bf16[128,2048]{1,0:T(8,128)(2,1)}), bf16[32,2048]{1,0:T(8,128)(2,1)}) %reduce-scatter.5.cloned.1.call-update) | async-done | bytes 131088 | tf_op jit(solution)/shard_map/reduce_scatter | solution.py:141
  392.7 1.7 add_convert_fusion
  (29 shorter events, 0.2 us)
Async XLA Ops:
  7.4 77.5 %copy-start = (bf16[512,2048]{1,0:T(8,128)(2,1)S(1)}, bf16[512,2048]{1,0:T(8,128)(2,1)}, u32[]{:S(2)}) copy-start(bf16[512,2048]{1,0:T(8,128)(2,1)} %param.23) | copy-start | bytes 6291460
  7.4 99.9 %reduce-scatter.3.cloned.1.call-start = ((), (), s32[]{:S(2)}) async-start(), calls=%async_computation.2 | async-start | bytes 655360 | tf_op jit(solution)/shard_map/reduce_scatter | solution.py:116
  73.3 1.8 copy-start.2
  75.1 2.7 copy-start.1
  80.0 1.8 copy-start.2
  81.8 2.7 copy-start.1
  84.9 22.4 %copy-start.4 = (bf16[128,2048]{1,0:T(8,128)(2,1)S(1)}, bf16[128,2048]{1,0:T(8,128)(2,1)}, u32[]{:S(2)}) copy-start(bf16[128,2048]{1,0:T(8,128)(2,1)} %param.15) | copy-start | bytes 1572868
  86.2 22.2 %copy-start.5 = (f32[2048]{0:T(1024)S(1)}, f32[2048]{0:T(1024)}, u32[]{:S(2)}) copy-start(f32[2048]{0:T(1024)} %param.24) | copy-start | bytes 24580
  86.2 94.1 %all-gather.4.cloned.1.call-start = ((), (), s32[]{:S(2)}) async-start(), calls=%async_computation.3 | async-start | bytes 6488064 | tf_op jit(solution)/shard_map/all_gather | solution.py:127
  86.8 185.9 %all-gather.6.cloned.1.call-start = ((), (), s32[]{:S(2)}) async-start(), calls=%async_computation.4 | async-start | bytes 6488064 | tf_op jit(solution)/shard_map/all_gather | solution.py:132
  87.4 278.3 %all-gather.8.cloned.1.call-start = ((), (), s32[]{:S(2)}) async-start(), calls=%async_computation.5 | async-start | bytes 6488064 | tf_op jit(solution)/shard_map/all_gather | solution.py:138
  88.0 304.8 %reduce-scatter.5.cloned.1.call-start = ((), (), s32[]{:S(2)}) async-start(), calls=%async_computation.6 | async-start | bytes 655360 | tf_op jit(solution)/shard_map/reduce_scatter | solution.py:141
  184.0 208.8 %copy-start.3 = (bf16[32,2048]{1,0:T(8,128)(2,1)S(1)}, bf16[32,2048]{1,0:T(8,128)(2,1)}, u32[]{:S(2)}) copy-start(bf16[32,2048]{1,0:T(8,128)(2,1)} %reduce-scatter.3.cloned.1.call-done) | copy-start | bytes 393220
Sparse Core Ops, SparseCore 0:
  86.3 20.9 reduce-scatter.2
  372.9 19.8 reduce-scatter.4
Sparse Core Ops, SparseCore 1:
  88.9 91.4 all-gather.3
  182.4 90.2 all-gather.5
  274.6 91.0 all-gather.7
where the time goes:
time: 402 us
  waiting for transfers between devices  287 us (71%)
  blocking collectives  65.7 us (16%)
  matrix products  24.5 us (6%)
  between operations  15.2 us (4%)
  other arithmetic  7.31 us (2%)
    all_gather x1, waiting for transfers between devices, per_device(): lax.all_gather(down_weight, 'sp', axis=1, tiled=True)  93 us
    all_gather x1, waiting for transfers between devices, per_device(): lax.all_gather(up_weight, 'sp', axis=0, tiled=True)  88.7 us
    all_gather x1, waiting for transfers between devices, per_device(): lax.all_gather(gate_weight, 'sp', axis=0, tiled=True)  64.3 us
    all_gather x1, blocking collectives, per_device(): latent_piece = lax.all_gather(latent, 'sp', axis=0, tiled=True)  31.3 us
    all_gather x1, blocking collectives, per_device(): pos_piece = lax.all_gather(key_rot, 'sp', axis=0, tiled=True)  27.8 us
    reduce_scatter x1, waiting for transfers between devices, per_device(): lax.psum_scatter(terms.astype(jnp.bfloat16), 'tp', scatter_dimension=0, t...  20 us
    reduce_scatter x1, waiting for transfers between devices, per_device(): lax.psum_scatter(jnp.dot(attended, out_weight, preferred_element_type=jnp...  19.3 us
  transfers between devices with their start and end apart: 5, of which 5 were waited for; matrix products, arithmetic and copies ran while one was open for 1% of the time, Pallas kernels for 0%

commit v1 on v0

--- a/solution.py
+++ b/solution.py
@@ -1,8 +1,11 @@
+import functools
 import math
 
 import jax
 import jax.numpy as jnp
 from jax import lax
+from jax.experimental import pallas as pl
+from jax.experimental.pallas import tpu as pltpu
 from jax.sharding import PartitionSpec as P
 
 NOPE = 64
@@ -23,7 +26,7 @@
     return values * lax.rsqrt(jnp.mean(values * values, axis=-1, keepdims=True) + 1e-06) * gain
 
 
-def per_device(
+def plain_layer(
     resid_in,
     query_plain,
     query_turn,
@@ -143,6 +146,430 @@
     ).astype(jnp.float32)
     return (middle + 0.5 * down_sum).astype(jnp.bfloat16)
 
+MESH = pl.DeviceIdType.MESH
+BF = jnp.bfloat16
+F32 = jnp.float32
+BY_LAST = (((1,), (1,)), ((), ()))
+
+
+def turn(values, cosine, sine):
+    width = values.shape[-1]
+    half = ROPE // 2
+    lane = lax.broadcasted_iota(jnp.int32, values.shape, 1) % ROPE
+    swapped = jnp.where(lane < half, pltpu.roll(values, width - half, 1), pltpu.roll(values, half, 1))
+    return values * cosine + swapped * sine
+
+
+def layer_kernel(
+    sizes,
+    resid_ref,
+    query_ref,
+    turn_ref,
+    latent_ref,
+    shared_ref,
+    cos_ref,
+    sin_ref,
+    lgain_ref,
+    kup_ref,
+    vup_ref,
+    ow_ref,
+    mgain_ref,
+    send_ref,
+    out_ref,
+    kv_buf,
+    key_buf,
+    val_buf,
+    att_buf,
+    mix_buf,
+    mixb_buf,
+    mixr_buf,
+    mid_buf,
+    w_buf,
+    n_buf,
+    p_buf,
+    r1_buf,
+    acc_buf,
+    r_buf,
+    w_ssem,
+    w_rsem,
+    w_lsem,
+    l_ssem,
+    l_rsem,
+    f_ssem,
+    f_rsem,
+    m_ssem,
+    m_rsem,
+    a_ssem,
+    a_rsem,
+    d_ssem,
+    d_rsem,
+    c_ssem,
+    c_rsem,
+    s_ssem,
+    s_rsem,
+):
+    sp, tp, zs, ys, xs = sizes
+    s = lax.axis_index("sp")
+    t = lax.axis_index("tp")
+    core = t % 2
+    other = t + 1 - 2 * core
+    me = (s // ys, s % ys, t // 2)
+    dims = (zs, ys, xs)
+    rows = latent_ref.shape[0]
+    part = rows // tp
+    hid = send_ref.shape[1] // 3
+    cols = send_ref.shape[2]
+    kv_width = latent_ref.shape[1]
+
+    def remote(src, dst, ssem, rsem, dev):
+        return pltpu.make_async_remote_copy(
+            src_ref=src, dst_ref=dst, send_sem=ssem, recv_sem=rsem, device_id=dev, device_id_type=MESH
+        )
+
+    sends = []
+
+    lat = latent_ref[...].astype(F32)
+    lat = lat * lax.rsqrt(jnp.mean(lat * lat, axis=-1, keepdims=True) + 1e-06) * lgain_ref[...]
+    cosine = cos_ref[...]
+    sine = sin_ref[...]
+    half_rows = rows // 2
+    own_lat = lat.astype(BF)
+    own_key = turn(shared_ref[...].astype(F32), cosine, sine).astype(BF)
+    for half in range(2):
+        part_of = slice(half * half_rows, (half + 1) * half_rows)
+        kv_buf[0, half, :, :kv_width] = own_lat[part_of]
+        kv_buf[0, half, :, kv_width:] = own_key[part_of]
+    for k in range(1, sp):
+        cp = remote(kv_buf.at[0, core], kv_buf.at[k, core], l_ssem.at[k], l_rsem.at[k], ((s + k) % sp, t))
+        cp.start()
+        sends.append(cp)
+    w_slot = w_buf.at[:, pl.ds(pl.multiple_of(s * cols, cols), cols)]
+    keep = pltpu.make_async_copy(send_ref.at[s], w_slot, w_lsem)
+    keep.start()
+    for k in range(1, sp):
+        dest = (s + k) % sp
+        cp = remote(send_ref.at[dest], w_slot, w_ssem.at[k], w_rsem.at[k], (dest, t))
+        cp.start()
+        sends.append(cp)
+
+    def make_kv(k):
+        piece = kv_buf[k].reshape(rows, kv_buf.shape[3])
+        piece_lat = piece[:, :kv_width]
+        key_buf[k * rows:(k + 1) * rows, :] = jnp.dot(
+            piece_lat, kup_ref[...], preferred_element_type=F32
+        ).astype(BF)
+        val_buf[k * rows:(k + 1) * rows, :] = jnp.dot(
+            piece_lat, vup_ref[...], preferred_element_type=F32
+        ).astype(BF)
+
+    make_kv(0)
+    query_rot = turn(
+        turn_ref[...].astype(F32),
+        jnp.concatenate([cosine] * (turn_ref.shape[1] // cosine.shape[1]), axis=1),
+        jnp.concatenate([sine] * (turn_ref.shape[1] // cosine.shape[1]), axis=1),
+    ).astype(BF)
+    for k in range(1, sp):
+        remote(kv_buf.at[k, core], kv_buf.at[k, core], l_ssem.at[k], l_rsem.at[k], (s, other)).wait_recv()
+        cp = remote(kv_buf.at[k, core], kv_buf.at[k, core], f_ssem.at[k], f_rsem.at[k], (s, other))
+        cp.start()
+        sends.append(cp)
+    for k in range(1, sp):
+        remote(
+            kv_buf.at[k, 1 - core], kv_buf.at[k, 1 - core], f_ssem.at[k], f_rsem.at[k], (s, other)
+        ).wait_recv()
+        make_kv(k)
+
+    scale = (NOPE + ROPE) ** (-0.5)
+    all_rot = kv_buf[...].reshape(sp * rows, kv_buf.shape[3])[:, kv_width:]
+    lane = lax.broadcasted_iota(jnp.int32, (rows, 128), 1)
+    for pair in range(query_ref.shape[1] // 128):
+        span = slice(pair * 128, (pair + 1) * 128)
+        keys = jnp.concatenate([key_buf[:, span], all_rot], axis=1)
+        vals = val_buf[:, span]
+        results = []
+        for inner in range(2):
+            head = pair * 2 + inner
+            tile = head * ROPE // 128
+            group = head % (128 // ROPE)
+            q_plain = jnp.where(lane // NOPE == inner, query_ref[:, span], jnp.zeros((), BF))
+            q_turn = jnp.where(
+                lane // ROPE == group, query_rot[:, tile * 128:(tile + 1) * 128], jnp.zeros((), BF)
+            )
+            score = lax.dot_general(
+                jnp.concatenate([q_plain, q_turn], axis=1), keys, BY_LAST, preferred_element_type=F32
+            ) * scale
+            top = jnp.max(score, axis=-1, keepdims=True)
+            expo = jnp.exp(score - top)
+            total = jnp.sum(expo, axis=-1, keepdims=True)
+            results.append(jnp.dot(expo.astype(BF), vals, preferred_element_type=F32) / total)
+        att_buf[:, span] = jnp.where(lane < V, results[0], results[1]).astype(BF)
+
+    mix_buf[...] = jnp.dot(att_buf[...], ow_ref[...], preferred_element_type=F32)
+    mixb_buf[...] = mix_buf[...].astype(BF).reshape(mixb_buf.shape)
+    for j in range(1, tp):
+        dest = (t + j) % tp
+        cp = remote(mixb_buf.at[dest], mixr_buf.at[j], m_ssem.at[j], m_rsem.at[j], (s, dest))
+        cp.start()
+        sends.append(cp)
+    own_rows = pl.ds(pl.multiple_of(t * part, part), part)
+    mid = resid_ref[own_rows, :].astype(F32) + mix_buf[own_rows, :]
+    for j in range(1, tp):
+        remote(mixb_buf.at[0], mixr_buf.at[j], m_ssem.at[j], m_rsem.at[j], (s, other)).wait_recv()
+        mid = mid + mixr_buf[j].astype(F32)
+    mid_buf[...] = mid
+    normed = mid * lax.rsqrt(jnp.mean(mid * mid, axis=-1, keepdims=True) + 1e-06) * mgain_ref[...]
+    index_of = lambda place: (place[0] * ys + place[1]) * xs + place[2]
+    mine = index_of(me)
+    n_buf[mine, core] = normed.astype(BF)
+
+    def shifted(offset):
+        return tuple((m + o) % n for m, o, n in zip(me, offset, dims))
+
+    def device(offset):
+        z, y, x = shifted(offset)
+        return (z * ys + y, x * 2 + core)
+
+    def along(d, k):
+        return tuple(k if i == d else 0 for i in range(3))
+
+    def plus(offset, d, k):
+        return tuple((o + k) % dims[d] if i == d else o for i, o in enumerate(offset))
+
+    def gather(order):
+        held = [((0, 0, 0), -1)]
+        out = []
+        for stage, d in enumerate(order):
+            for offset, _ in list(held):
+                for k in range(1, dims[d]):
+                    held.append((plus(offset, d, k), stage))
+        for offset, stage in held:
+            block = n_buf.at[index_of(shifted(offset)), core]
+            if stage >= 0:
+                i = index_of(offset)
+                remote(block, block, a_ssem.at[i], a_rsem.at[i], (s, other)).wait_recv()
+            for d in order[stage + 1:]:
+                for k in range(1, dims[d]):
+                    i = index_of(plus(offset, d, -k))
+                    cp = remote(block, block, a_ssem.at[i], a_rsem.at[i], device(along(d, k)))
+                    cp.start()
+                    out.append(cp)
+            i = index_of(offset)
+            cp = remote(block, block, d_ssem.at[i], d_rsem.at[i], (s, other))
+            cp.start()
+            out.append(cp)
+        for offset, _ in held:
+            i = index_of(offset)
+            block = n_buf.at[index_of(shifted(offset)), 1 - core]
+            remote(block, block, d_ssem.at[i], d_rsem.at[i], (s, other)).wait_recv()
+        for cp in out:
+            cp.wait_send()
+
+    @pl.when(core == 0)
+    def _():
+        gather((0, 1, 2))
+
+    @pl.when(core == 1)
+    def _():
+        gather((2, 0, 1))
+
+    keep.wait()
+    for k in range(1, sp):
+        remote(w_buf.at[:, :cols], w_buf.at[:, :cols], w_ssem.at[k], w_rsem.at[k], (s, other)).wait_recv()
+
+    groups = n_buf.shape[0]
+    step = groups // c_ssem.shape[0]
+
+    def chunk(g, carry):
+        some = pl.ds(g * step, step)
+        block = n_buf[some].reshape(step * 2 * part, n_buf.shape[3])
+        gate = lax.dot_general(block, w_buf[:hid], BY_LAST, preferred_element_type=F32)
+        up = lax.dot_general(block, w_buf[hid:2 * hid], BY_LAST, preferred_element_type=F32)
+        hidden = (gate / (1.0 + jnp.exp(-gate)) * up).astype(BF)
+        down = jnp.dot(hidden, w_buf[2 * hid:], preferred_element_type=F32)
+        p_buf[some] = down.astype(BF).reshape(step, 2, part, n_buf.shape[3])
+        remote(p_buf.at[some, 1 - core], r1_buf.at[some], c_ssem.at[g], c_rsem.at[g], (s, other)).start()
+        return carry
+
+    lax.fori_loop(0, c_ssem.shape[0], chunk, 0)
+
+    def join(g, carry):
+        some = pl.ds(g * step, step)
+        remote(p_buf.at[some, 1 - core], r1_buf.at[some], c_ssem.at[g], c_rsem.at[g], (s, other)).wait()
+        acc_buf[some] = (p_buf[some, core].astype(F32) + r1_buf[some].astype(F32)).astype(BF)
+        return carry
+
+    lax.fori_loop(0, c_ssem.shape[0], join, 0)
+
+    def scatter(order):
+        out = []
+        live = [(0, 0, 0)]
+        for d in order:
+            live = [plus(o, d, k) for o in live for k in range(dims[d])]
+        for stage, d in enumerate(order):
+            for offset in live:
+                k = offset[d]
+                if k:
+                    i = index_of(plus(plus(offset, d, -k), d, -k))
+                    cp = remote(
+                        acc_buf.at[index_of(shifted(offset))],
+                        r_buf.at[i],
+                        s_ssem.at[i],
+                        s_rsem.at[i],
+                        device(along(d, k)),
+                    )
+                    cp.start()
+                    out.append(cp)
+            live = [o for o in live if o[d] == 0]
+            last = stage == len(order) - 1
+            for offset in live:
+                b = index_of(shifted(offset))
+                value = acc_buf[b].astype(F32)
+                for k in range(1, dims[d]):
+                    i = index_of(plus(offset, d, k))
+                    remote(r_buf.at[i], r_buf.at[i], s_ssem.at[i], s_rsem.at[i], (s, other)).wait_recv()
+                    value = value + r_buf[i].astype(F32)
+                if last:
+                    out_ref[...] = (mid_buf[...] + 0.5 * value).astype(BF)
+                else:
+                    acc_buf[b] = value.astype(BF)
+        for cp in out:
+            cp.wait_send()
+
+    @pl.when(core == 0)
+    def _():
+        scatter((2, 1, 0))
+
+    @pl.when(core == 1)
+    def _():
+        scatter((1, 0, 2))
+
+    for cp in sends:
+        cp.wait_send()
+
+
+def fused_layer(
+    zs,
+    resid_in,
+    query_plain,
+    query_turn,
+    latent_raw,
+    shared_key,
+    latent_gain,
+    key_up,
+    value_up,
+    out_weight,
+    mixer_gain,
+    gate_weight,
+    up_weight,
+    down_weight,
+):
+    sp = lax.axis_size("sp")
+    tp = lax.axis_size("tp")
+    ys = sp // zs
+    xs = tp // 2
+    rows, width = resid_in.shape
+    part = rows // tp
+    hid = down_weight.shape[0] // sp
+    cols = down_weight.shape[1]
+    kv = latent_raw.shape[1]
+    heads_width = query_plain.shape[1]
+    position = (lax.axis_index("sp") * rows + jnp.arange(rows, dtype=jnp.int32)).astype(F32)
+    inverse = 10000.0 ** (-jnp.arange(0, ROPE, 2, dtype=F32) / ROPE)
+    inverse_lanes = jnp.tile(inverse, 128 * 2 // ROPE)
+    angles = position[:, None] * inverse_lanes[None, :]
+    sign = jnp.where(jnp.arange(128) % ROPE < ROPE // 2, -1.0, 1.0).astype(F32)
+    cosine = jnp.cos(angles)
+    sine = jnp.sin(angles) * sign[None, :]
+    to_send = jnp.concatenate(
+        [
+            gate_weight.T.reshape(sp, hid, cols),
+            up_weight.T.reshape(sp, hid, cols),
+            down_weight.reshape(sp, hid, cols),
+        ],
+        axis=1,
+    )
+    groups = zs * ys * xs
+    chunks = math.gcd(groups, 4)
+    dma = pltpu.SemaphoreType.DMA
+    vmem = lambda *shape: pltpu.VMEM(shape, BF)
+    return pl.pallas_call(
+        functools.partial(layer_kernel, (sp, tp, zs, ys, xs)),
+        out_shape=jax.ShapeDtypeStruct((part, width), BF),
+        in_specs=[pl.BlockSpec(memory_space=pltpu.VMEM)] * 13,
+        out_specs=pl.BlockSpec(memory_space=pltpu.VMEM),
+        scratch_shapes=[
+            vmem(sp, 2, rows // 2, kv + 128),
+            vmem(sp * rows, heads_width),
+            vmem(sp * rows, heads_width),
+            vmem(rows, heads_width),
+            pltpu.VMEM((rows, width), F32),
+            vmem(tp, part, width),
+            vmem(tp, part, width),
+            pltpu.VMEM((part, width), F32),
+            vmem(3 * hid, width),
+            vmem(groups, 2, part, width),
+            vmem(groups, 2, part, width),
+            vmem(groups, part, width),
+            vmem(groups, part, width),
+            vmem(groups, part, width),
+            dma((sp,)),
+            dma((sp,)),
+            dma,
+            dma((sp,)),
+            dma((sp,)),
+            dma((sp,)),
+            dma((sp,)),
+            dma((tp,)),
+            dma((tp,)),
+            dma((groups,)),
+            dma((groups,)),
+            dma((groups,)),
+            dma((groups,)),
+            dma((chunks,)),
+            dma((chunks,)),
+            dma((groups,)),
+            dma((groups,)),
+        ],
+        compiler_params=pltpu.CompilerParams(has_side_effects=True, vmem_limit_bytes=60 * 1024 * 1024),
+    )(
+        resid_in,
+        query_plain,
+        query_turn,
+        latent_raw,
+        jnp.tile(shared_key, (1, 128 // ROPE)),
+        cosine,
+        sine,
+        latent_gain[None, :],
+        key_up,
+        value_up,
+        out_weight,
+        mixer_gain[None, :],
+        to_send,
+    )
+
+
+def per_device(*arrays):
+    resid_in, query_plain, query_turn, latent_raw = arrays[:4]
+    down_weight = arrays[-1]
+    sp = lax.axis_size("sp")
+    tp = lax.axis_size("tp")
+    rows = resid_in.shape[0]
+    fits = (
+        sp % 2 == 0
+        and tp % 2 == 0
+        and rows % (32 * tp) == 0
+        and down_weight.shape[0] % (16 * sp) == 0
+        and down_weight.shape[1] % 128 == 0
+        and latent_raw.shape[1] % 128 == 0
+        and query_plain.shape[1] % 128 == 0
+        and query_turn.shape[1] % 128 == 0
+        and rows * sp <= 1024
+        and sp * tp <= 32
+    )
+    if fits:
+        return fused_layer(sp // 2, *arrays)
+    return plain_layer(*arrays)
+
 
 def solution(mesh):
     return jax.shard_map(

time: 402 us -> 146 us (0.36)
  the two profiles are of different devices: /device:TPU:0 before, /device:TPU:27 now
where the time goes in v1:
time: 146 us; the launch traced here: 145 us
  Pallas kernels  138 us (95%)
  local copies, waits for them, and re-layouts  5.14 us (4%)
  other arithmetic  2.5 us (2%)
    pallas_call x1, Pallas kernels, fused_layer(): pl.pallas_call(functools.partial(layer_kernel, (sp, tp, zs, ys, xs)), out...  138 us

profile of v1, /device:TPU:27, one launch (start us, length us, event | category | flops | bytes accessed | tf_op | source)
XLA Modules:
  0.0 145.5 jit_solution(17050935057582468181)
XLA Ops:
  0.0 0.0 copy-start
  0.0 0.1 mul.36
  0.1 1.0 fusion
  1.1 1.4 copy.17
  2.5 1.4 copy.18
  3.9 0.0 copy-done
  3.9 0.0 copy-start.1
  3.9 1.5 %pad_maximum_fusion.send_ref = bf16[8,528,256]{2,1,0:T(8,128)(2,1)} fusion(bf16[8,176,256]{2,1,0:T(8,128)(2,1)S(1)} %bitcast.12, bf16[8,176,256]{2,1,0:T(8,128)(2,1)S(1)} %bitcast.9, bf16[8,176,256]{2,1,0:T(8,128)(2,1)S(1)} %bitcast.8), kind=kLoop, calls=%fused_computation | loop fusion | flops 6488064 | bytes 4325376 | tf_op jit(solution)/shard_map/concatenate | solution.py:483
  5.4 0.0 copy-done.1
  5.4 0.7 copy.19.shared_ref
  6.1 137.8 %shard_map.127 = bf16[32,2048]{1,0:T(8,128)(2,1)} custom-call(bf16[128,2048]{1,0:T(8,128)(2,1)} %resid_ref.1, bf16[128,512]{1,0:T(8,128)(2,1)} %query_ref.1, bf16[128,256]{1,0:T(8,128)(2,1)} %turn_ref.1, bf16[128,256]{1,0:T(8,128)(2,1)} %latent_ref.1, bf16[128,128]{1,0:T(8,128)(2,1)} %copy.19.shared_ref, f32[128,128]{1,0:T(8,128)} %get-tuple-element.6.cos_ref, ...), custom_call_target="tpu_custom_call" | custom-call | tf_op jit(solution)/shard_map/pallas_call | solution.py:495
  143.9 1.6 %copy.21 = bf16[32,2048]{1,0:T(8,128)(2,1)} copy(bf16[32,2048]{1,0:T(8,128)(2,1)} %shard_map.127) | data formatting | bytes 262144
  (5 shorter events, 0.0 us)
Async XLA Ops:
  0.0 3.9 %copy-start = (bf16[1408,256]{1,0:T(8,128)(2,1)S(1)}, bf16[1408,256]{1,0:T(8,128)(2,1)}, u32[]{:S(2)}) copy-start(bf16[1408,256]{1,0:T(8,128)(2,1)} %param.25) | copy-start | bytes 2162692
  3.9 1.5 %copy-start.1 = (bf16[128,32]{0,1:T(8,128)(2,1)S(1)}, bf16[128,32]{0,1:T(8,128)(2,1)}, u32[]{:S(2)}) copy-start(bf16[128,32]{0,1:T(8,128)(2,1)} %param.17) | copy-start | bytes 24580

commit v2 on v1

--- a/solution.py
+++ b/solution.py
@@ -174,7 +174,9 @@
     vup_ref,
     ow_ref,
     mgain_ref,
-    send_ref,
+    gate_ref,
+    up_ref,
+    down_ref,
     out_ref,
     kv_buf,
     key_buf,
@@ -208,17 +210,22 @@
     s_ssem,
     s_rsem,
 ):
-    sp, tp, zs, ys, xs = sizes
+    sp, tp, dims = sizes
+    axes = range(len(dims))
+    ring_dims, tp_dims = dims[:-1], dims[-1]
     s = lax.axis_index("sp")
     t = lax.axis_index("tp")
     core = t % 2
     other = t + 1 - 2 * core
-    me = (s // ys, s % ys, t // 2)
-    dims = (zs, ys, xs)
+    me = ()
+    rest = s
+    for size in reversed(ring_dims):
+        me = (rest % size,) + me
+        rest = rest // size
+    me = me + (t // 2,)
     rows = latent_ref.shape[0]
     part = rows // tp
-    hid = send_ref.shape[1] // 3
-    cols = send_ref.shape[2]
+    hid, cols = gate_ref.shape[1:]
     kv_width = latent_ref.shape[1]
 
     def remote(src, dst, ssem, rsem, dev):
@@ -243,14 +250,61 @@
         cp = remote(kv_buf.at[0, core], kv_buf.at[k, core], l_ssem.at[k], l_rsem.at[k], ((s + k) % sp, t))
         cp.start()
         sends.append(cp)
-    w_slot = w_buf.at[:, pl.ds(pl.multiple_of(s * cols, cols), cols)]
-    keep = pltpu.make_async_copy(send_ref.at[s], w_slot, w_lsem)
-    keep.start()
-    for k in range(1, sp):
-        dest = (s + k) % sp
-        cp = remote(send_ref.at[dest], w_slot, w_ssem.at[k], w_rsem.at[k], (dest, t))
-        cp.start()
-        sends.append(cp)
+    def index_of(place):
+        index = 0
+        for p, size in zip(place, dims):
+            index = index * size + p
+        return index
+
+    def shifted(offset):
+        return tuple((m + o) % n for m, o, n in zip(me, offset, dims))
+
+    def device(offset):
+        place = shifted(offset)
+        ring = 0
+        for p, size in zip(place, ring_dims):
+            ring = ring * size + p
+        return (ring, place[-1] * 2 + core)
+
+    def along(d, k):
+        return tuple(k if i == d else 0 for i in axes)
+
+    def plus(offset, d, k):
+        return tuple((o + k) % dims[d] if i == d else o for i, o in enumerate(offset))
+
+    def offsets(sizes_of):
+        found = [()]
+        for size in sizes_of:
+            found = [f + (k,) for f in found for k in range(size)]
+        return found
+
+    parts_of_w = (gate_ref, up_ref, down_ref)
+
+    def w_slot(which):
+        return w_buf.at[which * hid:(which + 1) * hid, pl.ds(pl.multiple_of(s * cols, cols), cols)]
+
+    keeps = [
+        pltpu.make_async_copy(ref.at[s], w_slot(which), w_lsem.at[which])
+        for which, ref in enumerate(parts_of_w)
+    ]
+    for keep in keeps:
+        keep.start()
+    ring = sorted(offsets(ring_dims)[1:], reverse=True)
+    late = [[o for o in ring if o[0]][-1], ring[-1]]
+    early = [o for o in ring if o not in late]
+
+    def send_weights(some, out):
+        for offset in some:
+            dest = device(offset + (0,))
+            i = index_of(offset + (0,)) // tp_dims
+            for which, ref in enumerate(parts_of_w):
+                cp = remote(
+                    ref.at[dest[0]], w_slot(which), w_ssem.at[which, i], w_rsem.at[which, i], dest
+                )
+                cp.start()
+                out.append(cp)
+
+    send_weights(early, sends)
 
     def make_kv(k):
         piece = kv_buf[k].reshape(rows, kv_buf.shape[3])
@@ -318,25 +372,11 @@
         mid = mid + mixr_buf[j].astype(F32)
     mid_buf[...] = mid
     normed = mid * lax.rsqrt(jnp.mean(mid * mid, axis=-1, keepdims=True) + 1e-06) * mgain_ref[...]
-    index_of = lambda place: (place[0] * ys + place[1]) * xs + place[2]
     mine = index_of(me)
     n_buf[mine, core] = normed.astype(BF)
 
-    def shifted(offset):
-        return tuple((m + o) % n for m, o, n in zip(me, offset, dims))
-
-    def device(offset):
-        z, y, x = shifted(offset)
-        return (z * ys + y, x * 2 + core)
-
-    def along(d, k):
-        return tuple(k if i == d else 0 for i in range(3))
-
-    def plus(offset, d, k):
-        return tuple((o + k) % dims[d] if i == d else o for i, o in enumerate(offset))
-
     def gather(order):
-        held = [((0, 0, 0), -1)]
+        held = [((0,) * len(dims), -1)]
         out = []
         for stage, d in enumerate(order):
             for offset, _ in list(held):
@@ -357,6 +397,8 @@
             cp = remote(block, block, d_ssem.at[i], d_rsem.at[i], (s, other))
             cp.start()
             out.append(cp)
+            if stage < 0:
+                send_weights(late, out)
         for offset, _ in held:
             i = index_of(offset)
             block = n_buf.at[index_of(shifted(offset)), 1 - core]
@@ -364,63 +406,62 @@
         for cp in out:
             cp.wait_send()
 
-    @pl.when(core == 0)
-    def _():
-        gather((0, 1, 2))
-
-    @pl.when(core == 1)
-    def _():
-        gather((2, 0, 1))
-
-    keep.wait()
-    for k in range(1, sp):
-        remote(w_buf.at[:, :cols], w_buf.at[:, :cols], w_ssem.at[k], w_rsem.at[k], (s, other)).wait_recv()
-
-    groups = n_buf.shape[0]
-    step = groups // c_ssem.shape[0]
-
-    def chunk(g, carry):
-        some = pl.ds(g * step, step)
-        block = n_buf[some].reshape(step * 2 * part, n_buf.shape[3])
-        gate = lax.dot_general(block, w_buf[:hid], BY_LAST, preferred_element_type=F32)
-        up = lax.dot_general(block, w_buf[hid:2 * hid], BY_LAST, preferred_element_type=F32)
-        hidden = (gate / (1.0 + jnp.exp(-gate)) * up).astype(BF)
-        down = jnp.dot(hidden, w_buf[2 * hid:], preferred_element_type=F32)
-        p_buf[some] = down.astype(BF).reshape(step, 2, part, n_buf.shape[3])
-        remote(p_buf.at[some, 1 - core], r1_buf.at[some], c_ssem.at[g], c_rsem.at[g], (s, other)).start()
-        return carry
-
-    lax.fori_loop(0, c_ssem.shape[0], chunk, 0)
-
-    def join(g, carry):
-        some = pl.ds(g * step, step)
-        remote(p_buf.at[some, 1 - core], r1_buf.at[some], c_ssem.at[g], c_rsem.at[g], (s, other)).wait()
-        acc_buf[some] = (p_buf[some, core].astype(F32) + r1_buf[some].astype(F32)).astype(BF)
-        return carry
-
-    lax.fori_loop(0, c_ssem.shape[0], join, 0)
-
-    def scatter(order):
+    def feed_forward(order):
+        for keep in keeps:
+            keep.wait()
+        for i in range(1, sp):
+            for which in range(3):
+                piece = w_buf.at[which * hid:(which + 1) * hid, :cols]
+                remote(piece, piece, w_ssem.at[which, i], w_rsem.at[which, i], (s, other)).wait_recv()
         out = []
-        live = [(0, 0, 0)]
-        for d in order:
-            live = [plus(o, d, k) for o in live for k in range(dims[d])]
+        zero = (0,) * len(dims)
+        inner = offsets(dims[2:])
+        step = len(inner)
+        chunks = sorted(offsets(dims[:2]), key=lambda o: (o[1] == 0, o[0] == 0))
+
+        def send(offset, d):
+            i = index_of(plus(plus(offset, d, -offset[d]), d, -offset[d]))
+            cp = remote(
+                acc_buf.at[index_of(shifted(offset))], r_buf.at[i], s_ssem.at[i], s_rsem.at[i],
+                device(along(d, offset[d])),
+            )
+            cp.start()
+            out.append(cp)
+
+        def across(g, outer):
+            base = index_of(shifted(outer + zero[2:])[:2] + zero[2:])
+            some = pl.ds(base, step)
+            return some, remote(
+                p_buf.at[some, 1 - core], r1_buf.at[some], c_ssem.at[g], c_rsem.at[g], (s, other)
+            )
+
+        def join(g, outer):
+            some, cp = across(g, outer)
+            cp.wait()
+            acc_buf[some] = (p_buf[some, core].astype(F32) + r1_buf[some].astype(F32)).astype(BF)
+            for o in inner:
+                if (outer + o)[order[0]]:
+                    send(outer + o, order[0])
+
+        for g, outer in enumerate(chunks):
+            some, cp = across(g, outer)
+            block = n_buf[some].reshape(step * 2 * part, n_buf.shape[3])
+            gate = lax.dot_general(block, w_buf[:hid], BY_LAST, preferred_element_type=F32)
+            up = lax.dot_general(block, w_buf[hid:2 * hid], BY_LAST, preferred_element_type=F32)
+            hidden = (gate / (1.0 + jnp.exp(-gate)) * up).astype(BF)
+            down = jnp.dot(hidden, w_buf[2 * hid:], preferred_element_type=F32)
+            p_buf[some] = down.astype(BF).reshape(step, 2, part, n_buf.shape[3])
+            cp.start()
+            if g:
+                join(g - 1, chunks[g - 1])
+        join(len(chunks) - 1, chunks[-1])
+
+        live = [outer + o for outer in chunks for o in inner]
         for stage, d in enumerate(order):
-            for offset in live:
-                k = offset[d]
-                if k:
-                    i = index_of(plus(plus(offset, d, -k), d, -k))
-                    cp = remote(
-                        acc_buf.at[index_of(shifted(offset))],
-                        r_buf.at[i],
-                        s_ssem.at[i],
-                        s_rsem.at[i],
-                        device(along(d, k)),
-                    )
-                    cp.start()
-                    out.append(cp)
+            last = stage == len(order) - 1
             live = [o for o in live if o[d] == 0]
-            last = stage == len(order) - 1
+            if not last:
+                live = [o for o in live if o[order[stage + 1]]] + [o for o in live if not o[order[stage + 1]]]
             for offset in live:
                 b = index_of(shifted(offset))
                 value = acc_buf[b].astype(F32)
@@ -432,23 +473,26 @@
                     out_ref[...] = (mid_buf[...] + 0.5 * value).astype(BF)
                 else:
                     acc_buf[b] = value.astype(BF)
+                    if offset[order[stage + 1]]:
+                        send(offset, order[stage + 1])
         for cp in out:
             cp.wait_send()
 
     @pl.when(core == 0)
     def _():
-        scatter((2, 1, 0))
+        gather((0, 1, 2, 3))
+        feed_forward((3, 2, 1, 0))
 
     @pl.when(core == 1)
     def _():
-        scatter((1, 0, 2))
+        gather((0, 1, 3, 2))
+        feed_forward((2, 3, 1, 0))
 
     for cp in sends:
         cp.wait_send()
 
 
 def fused_layer(
-    zs,
     resid_in,
     query_plain,
     query_turn,
@@ -465,8 +509,7 @@
 ):
     sp = lax.axis_size("sp")
     tp = lax.axis_size("tp")
-    ys = sp // zs
-    xs = tp // 2
+    dims = (2, sp // 4, 2, tp // 2)
     rows, width = resid_in.shape
     part = rows // tp
     hid = down_weight.shape[0] // sp
@@ -480,22 +523,14 @@
     sign = jnp.where(jnp.arange(128) % ROPE < ROPE // 2, -1.0, 1.0).astype(F32)
     cosine = jnp.cos(angles)
     sine = jnp.sin(angles) * sign[None, :]
-    to_send = jnp.concatenate(
-        [
-            gate_weight.T.reshape(sp, hid, cols),
-            up_weight.T.reshape(sp, hid, cols),
-            down_weight.reshape(sp, hid, cols),
-        ],
-        axis=1,
-    )
-    groups = zs * ys * xs
-    chunks = math.gcd(groups, 4)
+    groups = sp * tp // 2
+    chunks = dims[0] * dims[1]
     dma = pltpu.SemaphoreType.DMA
     vmem = lambda *shape: pltpu.VMEM(shape, BF)
     return pl.pallas_call(
-        functools.partial(layer_kernel, (sp, tp, zs, ys, xs)),
+        functools.partial(layer_kernel, (sp, tp, dims)),
         out_shape=jax.ShapeDtypeStruct((part, width), BF),
-        in_specs=[pl.BlockSpec(memory_space=pltpu.VMEM)] * 13,
+        in_specs=[pl.BlockSpec(memory_space=pltpu.VMEM)] * 15,
         out_specs=pl.BlockSpec(memory_space=pltpu.VMEM),
         scratch_shapes=[
             vmem(sp, 2, rows // 2, kv + 128),
@@ -512,9 +547,9 @@
             vmem(groups, part, width),
             vmem(groups, part, width),
             vmem(groups, part, width),
-            dma((sp,)),
-            dma((sp,)),
-            dma,
+            dma((3, sp)),
+            dma((3, sp)),
+            dma((3,)),
             dma((sp,)),
             dma((sp,)),
             dma((sp,)),
@@ -544,7 +579,9 @@
         value_up,
         out_weight,
         mixer_gain[None, :],
-        to_send,
+        gate_weight.T.reshape(sp, hid, cols),
+        up_weight.T.reshape(sp, hid, cols),
+        down_weight.reshape(sp, hid, cols),
     )
 
 
@@ -555,7 +592,7 @@
     tp = lax.axis_size("tp")
     rows = resid_in.shape[0]
     fits = (
-        sp % 2 == 0
+        sp % 4 == 0
         and tp % 2 == 0
         and rows % (32 * tp) == 0
         and down_weight.shape[0] % (16 * sp) == 0
@@ -567,7 +604,7 @@
         and sp * tp <= 32
     )
     if fits:
-        return fused_layer(sp // 2, *arrays)
+        return fused_layer(*arrays)
     return plain_layer(*arrays)
 
 

time: 146 us -> 132 us (0.904)
  the two profiles are of different devices: /device:TPU:27 before, /device:TPU:0 now
where the time goes in v2:
time: 132 us
  Pallas kernels  124 us (94%)
  local copies, waits for them, and re-layouts  6.52 us (5%)
    pallas_call x1, Pallas kernels, fused_layer(): pl.pallas_call(functools.partial(layer_kernel, (sp, tp, dims)), out_shape...  124 us

profile of v2, /device:TPU:0, one launch (start us, length us, event | category | flops | bytes accessed | tf_op | source)
XLA Modules:
  0.0 131.8 jit_solution(12531490341485060627)
XLA Ops:
  0.0 0.0 copy-start
  0.0 0.1 mul.36
  0.1 0.8 tile.6
  0.9 0.7 copy.19.shared_ref
  1.6 1.0 fusion
  2.6 2.2 %copy.17 = bf16[1408,256]{1,0:T(8,128)(2,1)} copy(bf16[1408,256]{0,1:T(8,128)(2,1)} %bitcast.11) | data formatting | bytes 1441792 | tf_op jit(solution)/shard_map/transpose | solution.py:582
  4.8 0.0 copy-done
  4.8 1.1 copy.18
  6.0 124.3 %shard_map.127 = bf16[32,2048]{1,0:T(8,128)(2,1)} custom-call(bf16[128,2048]{1,0:T(8,128)(2,1)} %resid_ref.1, bf16[128,512]{1,0:T(8,128)(2,1)} %query_ref.1, bf16[128,256]{1,0:T(8,128)(2,1)} %turn_ref.1, bf16[128,256]{1,0:T(8,128)(2,1)} %latent_ref.1, bf16[128,128]{1,0:T(8,128)(2,1)} %copy.19.shared_ref, f32[128,128]{1,0:T(8,128)} %get-tuple-element.6.cos_ref, ...), custom_call_target="tpu_custom_call" | custom-call | tf_op jit(solution)/shard_map/pallas_call | solution.py:530
  130.3 1.6 %copy.21 = bf16[32,2048]{1,0:T(8,128)(2,1)} copy(bf16[32,2048]{1,0:T(8,128)(2,1)} %shard_map.127) | data formatting | bytes 262144
  (4 shorter events, 0.0 us)
Async XLA Ops:
  0.0 4.8 %copy-start = (bf16[256,1408]{1,0:T(8,128)(2,1)S(1)}, bf16[256,1408]{1,0:T(8,128)(2,1)}, u32[]{:S(2)}) copy-start(bf16[256,1408]{1,0:T(8,128)(2,1)} %param.24) | copy-start | bytes 2162692

commit v3 on v2

--- a/solution.py
+++ b/solution.py
@@ -290,14 +290,14 @@
     for keep in keeps:
         keep.start()
     ring = sorted(offsets(ring_dims)[1:], reverse=True)
-    late = [[o for o in ring if o[0]][-1], ring[-1]]
+    late = [o for o in ring if o[0]][-2:] + ring[-3:]
     early = [o for o in ring if o not in late]
 
     def send_weights(some, out):
-        for offset in some:
-            dest = device(offset + (0,))
-            i = index_of(offset + (0,)) // tp_dims
-            for which, ref in enumerate(parts_of_w):
+        for which, ref in enumerate(parts_of_w):
+            for offset in some:
+                dest = device(offset + (0,))
+                i = index_of(offset + (0,)) // tp_dims
                 cp = remote(
                     ref.at[dest[0]], w_slot(which), w_ssem.at[which, i], w_rsem.at[which, i], dest
                 )
@@ -397,7 +397,7 @@
             cp = remote(block, block, d_ssem.at[i], d_rsem.at[i], (s, other))
             cp.start()
             out.append(cp)
-            if stage < 0:
+            if stage == 0:
                 send_weights(late, out)
         for offset, _ in held:
             i = index_of(offset)
@@ -407,12 +407,14 @@
             cp.wait_send()
 
     def feed_forward(order):
-        for keep in keeps:
-            keep.wait()
-        for i in range(1, sp):
-            for which in range(3):
-                piece = w_buf.at[which * hid:(which + 1) * hid, :cols]
+        def arrived(which):
+            keeps[which].wait()
+            piece = w_buf.at[which * hid:(which + 1) * hid, :cols]
+            for i in range(1, sp):
                 remote(piece, piece, w_ssem.at[which, i], w_rsem.at[which, i], (s, other)).wait_recv()
+
+        arrived(0)
+        arrived(1)
         out = []
         zero = (0,) * len(dims)
         inner = offsets(dims[2:])
@@ -449,6 +451,8 @@
             gate = lax.dot_general(block, w_buf[:hid], BY_LAST, preferred_element_type=F32)
             up = lax.dot_general(block, w_buf[hid:2 * hid], BY_LAST, preferred_element_type=F32)
             hidden = (gate / (1.0 + jnp.exp(-gate)) * up).astype(BF)
+            if g == 0:
+                arrived(2)
             down = jnp.dot(hidden, w_buf[2 * hid:], preferred_element_type=F32)
             p_buf[some] = down.astype(BF).reshape(step, 2, part, n_buf.shape[3])
             cp.start()
@@ -485,7 +489,7 @@
 
     @pl.when(core == 1)
     def _():
-        gather((0, 1, 3, 2))
+        gather((0, 1, 2, 3))
         feed_forward((2, 3, 1, 0))
 
     for cp in sends:

time: 132 us -> 127 us (0.962)
  Pallas kernels: 124 us -> 119 us
    pallas_call x1, Pallas kernels: 124 us -> 119 us  [fused_layer(): pl.pallas_call(functools.partial(layer_kernel, (sp, tp, dims)), out_shape...]
where the time goes in v3:
time: 127 us
  Pallas kernels  119 us (94%)
  local copies, waits for them, and re-layouts  6.52 us (5%)
    pallas_call x1, Pallas kernels, fused_layer(): pl.pallas_call(functools.partial(layer_kernel, (sp, tp, dims)), out_shape...  119 us

profile of v3, /device:TPU:0, one launch (start us, length us, event | category | flops | bytes accessed | tf_op | source)
XLA Modules:
  0.0 126.7 jit_solution(2003506338798271580)
XLA Ops:
  0.0 0.0 copy-start
  0.0 0.1 mul.36
  0.1 0.8 tile.6
  0.9 0.7 copy.19.shared_ref
  1.6 1.0 fusion
  2.6 2.2 %copy.17 = bf16[1408,256]{1,0:T(8,128)(2,1)} copy(bf16[1408,256]{0,1:T(8,128)(2,1)} %bitcast.11) | data formatting | bytes 1441792 | tf_op jit(solution)/shard_map/transpose | solution.py:586
  4.8 0.0 copy-done
  4.8 1.1 copy.18
  6.0 119.2 %shard_map.127 = bf16[32,2048]{1,0:T(8,128)(2,1)} custom-call(bf16[128,2048]{1,0:T(8,128)(2,1)} %resid_ref.1, bf16[128,512]{1,0:T(8,128)(2,1)} %query_ref.1, bf16[128,256]{1,0:T(8,128)(2,1)} %turn_ref.1, bf16[128,256]{1,0:T(8,128)(2,1)} %latent_ref.1, bf16[128,128]{1,0:T(8,128)(2,1)} %copy.19.shared_ref, f32[128,128]{1,0:T(8,128)} %get-tuple-element.6.cos_ref, ...), custom_call_target="tpu_custom_call" | custom-call | tf_op jit(solution)/shard_map/pallas_call | solution.py:534
  125.2 1.6 %copy.21 = bf16[32,2048]{1,0:T(8,128)(2,1)} copy(bf16[32,2048]{1,0:T(8,128)(2,1)} %shard_map.127) | data formatting | bytes 262144
  (4 shorter events, 0.0 us)
Async XLA Ops:
  0.0 4.8 %copy-start = (bf16[256,1408]{1,0:T(8,128)(2,1)S(1)}, bf16[256,1408]{1,0:T(8,128)(2,1)}, u32[]{:S(2)}) copy-start(bf16[256,1408]{1,0:T(8,128)(2,1)} %param.24) | copy-start | bytes 2162692
